TPU v7x, 32 devices: a whole 2x2x4 slice. The times are simulated.
32 devices in a mesh: sp: 8 (over z, x), tp: 4 (over y, core).
Axes of the slice: x: 2, y: 2, z: 4, core: 2. Of those that a mesh axis runs over, the one named last changes fastest.
Arguments:
- conv_value: bfloat16 [4096, 1024], P('sp', 'tp'), may hold values from -6 to 6
- conv_gate: bfloat16 [4096, 1024], P('sp', 'tp'), may hold values from -9 to 9
- conv_weight: float32 [31, 1024], P(None, 'tp'), may hold values from -2.2 to 2.2
- conv_gain: float32 [1024], P('tp'), may hold values from 0.1 to 1.9
- conv_shift: float32 [1024], P('tp'), may hold values from -3 to 3
- out_weight: bfloat16 [1024, 2048], P('tp'), may hold values from -0.1875 to 0.1875
- residual: bfloat16 [4096, 2048], P('sp', 'tp'), may hold values from -10 to 10
- mix_gain: float32 [2048], P('tp'), may hold values from 0.1 to 1.9
- expert_ids: int32 [4096, 2], P('sp'), may hold values from 0 to 7, all different within a row; in each aligned block of 128 rows (0 to 127, 128 to 255, ...) at most 64 rows name the same one
- group_weight: float32 [4096], P('sp'), may hold values from 0.6 to 1
- score_gap: float32 [4096], P('sp'), may hold values from -0.8 to 0.8
- w_gate: bfloat16 [8, 2048, 1024], P('sp', None, 'tp'), may hold values from -0.125 to 0.125
- w_up: bfloat16 [8, 2048, 1024], P('sp', None, 'tp'), may hold values from -0.125 to 0.125
- w_down: bfloat16 [8, 1024, 2048], P('sp', 'tp'), may hold values from -0.1875 to 0.1875
Outputs:
- layer_out: bfloat16 [4096, 2048], P('sp', 'tp')
Inputs may be any that keep to these rules, and one draw needn't show every extreme that they name: `expert_ids`: the two experts of a position differ. In each aligned block of 512 // 4 positions no expert is named by more than 64 rows, a bound that some block reaches.
All inputs are finite; a program needn't handle non-finite values.
Results may differ from a plain program's by a relative error of at most 0.012.
Values may be sent and summed in bfloat16 or wider, within the bound.
A program may use at most 128 MiB of HBM per device.

v0:
```python
import jax
import jax.numpy as jnp
from jax import lax
from jax.sharding import PartitionSpec as P

D = 2048
CH = 1024


eps = 1e-06


def passed_along(value, axis, steps):
    count = lax.axis_size(axis)
    leading, last = (max(0, -steps), min(count, count - steps))
    return lax.ppermute(value, axis, [(source, source + steps) for source in range(leading, last)])


def shards(
    conv_value,
    conv_gate,
    conv_weight,
    conv_gain,
    conv_shift,
    out_weight,
    residual,
    mix_gain,
    expert_ids,
    group_weight,
    score_gap,
    w_gate,
    w_up,
    w_down,
):
    row_count = conv_value.shape[0]
    reach_rows = conv_weight.shape[0] - 1
    seq_devices = lax.axis_size("sp")
    tp_devices = lax.axis_size("tp")
    prev_value, prev_gate = passed_along(
        (conv_value[row_count - reach_rows :], conv_gate[row_count - reach_rows :]), "sp", 1
    )
    values = jnp.concatenate([prev_value, conv_value], axis=0).astype(jnp.float32)
    gate_pre = jnp.concatenate([prev_gate, conv_gate], axis=0).astype(jnp.float32)
    gated = values * jax.nn.sigmoid(gate_pre)
    convolved = jnp.zeros((row_count, conv_value.shape[1]), jnp.float32)
    for tap_index in range(reach_rows + 1):
        convolved = convolved + conv_weight[tap_index] * gated[tap_index : tap_index + row_count]
    row_sum, squares = lax.psum(
        (jnp.sum(convolved, axis=-1), jnp.sum(convolved * convolved, axis=-1)), "tp"
    )
    row_mean = (row_sum / CH)[:, None]
    row_var = (squares / CH)[:, None] - row_mean * row_mean
    normalized = (convolved - row_mean) * lax.rsqrt(row_var + eps) * conv_gain + conv_shift
    activated = jax.nn.silu(normalized).astype(jnp.bfloat16)
    partial_out = jnp.dot(activated, out_weight, preferred_element_type=jnp.float32)
    mixed = lax.psum_scatter(
        partial_out.astype(jnp.bfloat16), "tp", scatter_dimension=1, tiled=True
    ).astype(jnp.float32)
    middle = (residual.astype(jnp.float32) + mixed).astype(jnp.bfloat16)
    middle_wide = middle.astype(jnp.float32)
    row_sq = lax.psum(jnp.sum(middle_wide * middle_wide, axis=-1), "tp")
    normed = (middle_wide * lax.rsqrt(row_sq / D + eps)[:, None] * mix_gain).astype(jnp.bfloat16)
    quarter = row_count // tp_devices
    capacity = 4 * quarter // seq_devices
    expert_num = expert_ids.reshape(tp_devices, quarter * 2)
    onehot = (
        expert_num[:, :, None] == jnp.arange(seq_devices, dtype=jnp.int32)[None, None, :]
    ).astype(jnp.int32)
    before = jnp.cumsum(onehot, axis=1) - onehot
    ranking = jnp.sum(before * onehot, axis=-1)
    quarter_index = jnp.arange(tp_devices, dtype=jnp.int32)[:, None]
    slots = ((expert_num * tp_devices + quarter_index) * capacity + ranking).reshape(-1)
    own_rows = lax.all_to_all(normed, "tp", split_axis=0, concat_axis=1, tiled=True)
    my_index = lax.axis_index("tp")
    own_experts = lax.dynamic_slice_in_dim(expert_num, my_index, 1, 0)[0]
    own_rank = lax.dynamic_slice_in_dim(ranking, my_index, 1, 0)[0]
    own_slots = own_experts * capacity + own_rank
    token_of = jnp.arange(quarter * 2, dtype=jnp.int32) // 2
    outgoing = (
        jnp.zeros((seq_devices * capacity, D), jnp.bfloat16).at[own_slots].set(own_rows[token_of])
    )
    received = lax.all_to_all(
        outgoing.reshape(seq_devices, capacity, D), "sp", split_axis=0, concat_axis=0, tiled=True
    )
    gathered = lax.all_gather(received[:, None], "tp", axis=1, tiled=True)
    expert_in = gathered.reshape(-1, D)
    gate_part = jnp.dot(expert_in, w_gate[0], preferred_element_type=jnp.float32)
    up_part = jnp.dot(expert_in, w_up[0], preferred_element_type=jnp.float32)
    hidden = (jax.nn.silu(gate_part) * up_part).astype(jnp.bfloat16)
    partial_value = jnp.dot(hidden, w_down[0], preferred_element_type=jnp.float32)
    columns = lax.psum_scatter(
        partial_value.astype(jnp.bfloat16), "tp", scatter_dimension=1, tiled=True
    )
    col_count = columns.shape[1]
    returned = lax.all_to_all(
        columns.reshape(seq_devices, tp_devices * capacity, col_count),
        "sp",
        split_axis=0,
        concat_axis=0,
        tiled=True,
    )
    lookup = returned.reshape(-1, col_count)
    col_count = lookup.shape[1]
    picked = lookup[slots].reshape(row_count, 2, col_count).astype(jnp.float32)
    first_gate = group_weight * jax.nn.sigmoid(score_gap)
    second_gate = group_weight * jax.nn.sigmoid(-score_gap)
    result = middle_wide + first_gate[:, None] * picked[:, 0] + second_gate[:, None] * picked[:, 1]
    return result.astype(jnp.bfloat16)


def solution(mesh):
    return jax.shard_map(
        shards,
        mesh=mesh,
        in_specs=(
            P("sp", "tp"),
            P("sp", "tp"),
            P(None, "tp"),
            P("tp"),
            P("tp"),
            P("tp", None),
            P("sp", "tp"),
            P("tp"),
            P("sp", None),
            P("sp"),
            P("sp"),
            P("sp", None, "tp"),
            P("sp", None, "tp"),
            P("sp", "tp", None),
        ),
        out_specs=P("sp", "tp"),
        check_vma=False,
    )
```

profile of v0, /device:TPU:17, one launch (start us, length us, event | category | flops | bytes accessed | tf_op | source)
XLA Modules:
  0.0 358.2 jit_solution(2769100146873338767)
XLA Ops:
  7.4 3.1 collective-permute-start
  11.2 3.2 collective-permute-start.1
  16.6 1.2 divide_multiply_fusion
  17.8 2.4 fusion.59
  20.2 7.1 %all-reduce = (f32[512]{0:T(512)S(1)}, f32[512]{0:T(512)S(1)}) all-reduce(f32[512]{0:T(512)S(1)} %get-tuple-element.6, f32[512]{0:T(512)S(1)} %get-tuple-element.5), channel_id=1, replica_groups=mesh['sp'=8,'tp'=4] {'tp'}, use_global_device_ids=true, to_apply=%region_3.0 | all-reduce | flops 1024 | bytes 8192 | tf_op jit(solution)/shard_map/psum | solution.py:48
  27.4 2.1 convolution_convert_fusion.1
  30.6 2.3 reduce-window.6
  33.0 28.0 %reduce-scatter.3.cloned.1.call-done = bf16[512,512]{1,0:T(8,128)(2,1)} async-done(((bf16[512,2048]{1,0:T(8,128)(2,1)}), bf16[512,512]{1,0:T(8,128)(2,1)}) %reduce-scatter.3.cloned.1.call-update) | async-done | bytes 524304 | tf_op jit(solution)/shard_map/reduce_scatter | solution.py:56
  61.0 1.3 fusion.1
  62.3 5.9 %psum.23 = f32[512]{0:T(512)S(1)} all-reduce(f32[512]{0:T(512)S(1)} %fusion.1), channel_id=1, replica_groups=mesh['sp'=8,'tp'=4] {'tp'}, use_global_device_ids=true, to_apply=%region_9.10 | all-reduce | flops 512 | bytes 4096 | tf_op jit(solution)/shard_map/psum | solution.py:61
  68.2 2.0 fusion.3
  70.2 4.4 %all-to-all-start = ((bf16[4,128,512]{2,1,0:T(8,128)(2,1)}), bf16[4,128,512]{2,1,0:T(8,128)(2,1)S(1)}, u32[]{:S(2)}, u32[]{:S(2)}) async-start(bf16[4,128,512]{2,1,0:T(8,128)(2,1)} %bitcast.36), calls=%async_computation.1 | async-start | bytes 1048576 | tf_op jit(solution)/shard_map/all_to_all | solution.py:73
  74.9 7.5 %all-to-all-done = bf16[4,128,512]{2,1,0:T(8,128)(2,1)S(1)} async-done(((bf16[4,128,512]{2,1,0:T(8,128)(2,1)}), bf16[4,128,512]{2,1,0:T(8,128)(2,1)S(1)}, u32[]{:S(2)}, u32[]{:S(2)}) %all-to-all-start) | async-done | bytes 524320 | tf_op jit(solution)/shard_map/all_to_all | solution.py:73
  83.3 6.4 %scatter_custom_fusion = bf16[512,2048]{1,0:T(8,128)(2,1)S(1)} fusion(s32[256]{0:T(256)S(1)} %bitcast.130, bf16[128,2048]{1,0:T(8,128)(2,1)} %bitcast.93, s32[1024]{0:T(1024)S(1)} %pad_clamp_fusion, bf16[]{:T(256)} %constant.25.clone.1), kind=kCustom, calls=%fused_computation.23 | custom fusion | bytes 2097664 | tf_op jit(solution)/shard_map/scatter | solution.py:80
  89.7 51.3 %all_to_all.29 = bf16[8,64,2048]{2,1,0:T(8,128)(2,1)} all-to-all(bf16[8,64,2048]{2,1,0:T(8,128)(2,1)S(1)} %bitcast.90), channel_id=1, replica_groups=mesh['sp'=8,'tp'=4] {'sp'}, dimensions={0} | all-to-all | bytes 4194304 | tf_op jit(solution)/shard_map/all_to_all | solution.py:82
  141.2 59.3 %all-gather.3.cloned.1.call-done = bf16[8,256,2048]{2,1,0:T(8,128)(2,1)} async-done(((bf16[8,64,2048]{2,1,0:T(8,128)(2,1)}), bf16[8,256,2048]{2,1,0:T(8,128)(2,1)}) %all-gather.3.cloned.1.call-update) | async-done | bytes 8388624 | tf_op jit(solution)/shard_map/all_gather | solution.py:85
  200.5 7.2 %fusion.11 = f32[2048,256]{1,0:T(8,128)} fusion(bf16[2048,2048]{1,0:T(8,128)(2,1)} %bitcast.131, bf16[1,2048,256]{2,1,0:T(8,128)(2,1)S(1)} %copy-done.9), kind=kOutput, calls=%fused_computation.21 | convolution fusion | flops 2147483648 | bytes 11534336 | tf_op jit(solution)/shard_map/dot_general | solution.py:87
  207.7 13.1 %convolution_convert_fusion = bf16[2048,2048]{1,0:T(8,128)(2,1)} fusion(bf16[2048,2048]{1,0:T(8,128)(2,1)} %bitcast.132, f32[2048,256]{1,0:T(8,128)} %fusion.11, bf16[1,256,2048]{2,1,0:T(8,128)(2,1)S(1)} %copy-done, bf16[1,2048,256]{2,1,0:T(8,128)(2,1)S(1)} %copy-done.10), kind=kOutput, calls=%fused_computation.3 | convolution fusion | flops 4302307328 | bytes 20971520 | tf_op jit(solution)/shard_map/dot_general | solution.py:90
  220.8 70.8 %reduce-scatter.5.cloned.1.call-done = bf16[2048,512]{1,0:T(8,128)(2,1)} async-done(((bf16[2048,2048]{1,0:T(8,128)(2,1)}), bf16[2048,512]{1,0:T(8,128)(2,1)}) %reduce-scatter.5.cloned.1.call-update) | async-done | bytes 2097168 | tf_op jit(solution)/shard_map/reduce_scatter | solution.py:91
  291.6 5.6 %all-to-all-start.2 = ((bf16[8,256,512]{2,1,0:T(8,128)(2,1)}), bf16[8,256,512]{2,1,0:T(8,128)(2,1)S(1)}, u32[]{:S(2)}, u32[]{:S(2)}) async-start(bf16[8,256,512]{2,1,0:T(8,128)(2,1)} %bitcast.91), calls=%async_computation.4 | async-start | bytes 4194304 | tf_op jit(solution)/shard_map/all_to_all | solution.py:95
  297.7 43.8 %all-to-all-done.2 = bf16[8,256,512]{2,1,0:T(8,128)(2,1)S(1)} async-done(((bf16[8,256,512]{2,1,0:T(8,128)(2,1)}), bf16[8,256,512]{2,1,0:T(8,128)(2,1)S(1)}, u32[]{:S(2)}, u32[]{:S(2)}) %all-to-all-start.2) | async-done | bytes 2097184 | tf_op jit(solution)/shard_map/all_to_all | solution.py:95
  341.5 5.0 %gather_fusion = bf16[1024,512]{1,0:T(8,128)(2,1)} fusion(bf16[2048,512]{1,0:T(8,128)(2,1)S(1)} %bitcast.89, s32[1024]{0:T(1024)S(1)} %broadcast_clamp_fusion), kind=kCustom, calls=%fused_computation.1 | custom fusion | bytes 2101248 | tf_op jit(solution)/shard_map/gather | solution.py:104
  346.6 2.4 reshape.174
  349.0 1.6 fusion.61
  (64 shorter events, 7.9 us)
Async XLA Ops:
  6.5 201.1 %copy-start = (bf16[1,256,2048]{2,1,0:T(8,128)(2,1)S(1)}, bf16[1,256,2048]{2,1,0:T(8,128)(2,1)}, u32[]{:S(2)}) copy-start(bf16[1,256,2048]{2,1,0:T(8,128)(2,1)} %param.27) | copy-start | bytes 3145732
  6.5 54.5 %reduce-scatter.3.cloned.1.call-start = ((), (), s32[]{:S(2)}) async-start(), calls=%async_computation.5 | async-start | bytes 2621440 | tf_op jit(solution)/shard_map/reduce_scatter | solution.py:56
  7.4 9.0 %collective-permute-start = (bf16[30,256]{1,0:T(8,128)(2,1)S(1)}, bf16[30,256]{1,0:T(8,128)(2,1)S(1)}, u32[]{:S(2)}, u32[]{:S(2)}) collective-permute-start(bf16[30,256]{1,0:T(8,128)(2,1)S(1)} %slice.205), channel_id=1, source_target_pairs={{0,4},{4,8},{8,12},{12,16},{16,20},{20,24},{24,28},{1,5},{5,9},{9,... | collective-permute-start | bytes 46088 | tf_op jit(solution)/shard_map/ppermute | solution.py:16
  11.2 5.4 %collective-permute-start.1 = (bf16[30,256]{1,0:T(8,128)(2,1)S(1)}, bf16[30,256]{1,0:T(8,128)(2,1)S(1)}, u32[]{:S(2)}, u32[]{:S(2)}) collective-permute-start(bf16[30,256]{1,0:T(8,128)(2,1)S(1)} %slice.206), channel_id=1, source_target_pairs={{0,4},{4,8},{8,12},{12,16},{16,20},{20,24},{24,28},{1,5},{5,9},{9,... | collective-permute-start | bytes 46088 | tf_op jit(solution)/shard_map/ppermute | solution.py:16
  17.8 9.6 %copy-start.8 = (bf16[256,2048]{1,0:T(8,128)(2,1)S(1)}, bf16[256,2048]{1,0:T(8,128)(2,1)}, u32[]{:S(2)}) copy-start(bf16[256,2048]{1,0:T(8,128)(2,1)} %param.19) | copy-start | bytes 3145732
  17.8 9.5 %copy-start.11 = (f32[256]{0:T(256)S(1)}, f32[256]{0:T(256)}, u32[]{:S(2)}) copy-start(f32[256]{0:T(256)} %param.18) | copy-start | bytes 3076
  17.8 9.5 %copy-start.12 = (f32[256]{0:T(256)S(1)}, f32[256]{0:T(256)}, u32[]{:S(2)}) copy-start(f32[256]{0:T(256)} %param.17) | copy-start | bytes 3076
  29.5 0.7 copy-start.4
  29.5 31.5 %copy-start.1 = (bf16[512,512]{1,0:T(8,128)(2,1)S(1)}, bf16[512,512]{1,0:T(8,128)(2,1)}, u32[]{:S(2)}) copy-start(bf16[512,512]{1,0:T(8,128)(2,1)} %param.20) | copy-start | bytes 1572868
  29.5 38.7 %copy-start.5 = (f32[512]{0:T(512)S(1)}, f32[512]{0:T(512)}, u32[]{:S(2)}) copy-start(f32[512]{0:T(512)} %param.21) | copy-start | bytes 6148
  70.2 12.2 %all-to-all-start = ((bf16[4,128,512]{2,1,0:T(8,128)(2,1)}), bf16[4,128,512]{2,1,0:T(8,128)(2,1)S(1)}, u32[]{:S(2)}, u32[]{:S(2)}) async-start(bf16[4,128,512]{2,1,0:T(8,128)(2,1)} %bitcast.36), calls=%async_computation.1 | async-start | bytes 1048576 | tf_op jit(solution)/shard_map/all_to_all | solution.py:73
  74.6 125.9 %all-gather.3.cloned.1.call-start = ((), (), s32[]{:S(2)}) async-start(), calls=%async_computation.7 | async-start | bytes 10485760 | tf_op jit(solution)/shard_map/all_gather | solution.py:85
  141.0 59.5 %copy-start.9 = (bf16[1,2048,256]{2,1,0:T(8,128)(2,1)S(1)}, bf16[1,2048,256]{2,1,0:T(8,128)(2,1)}, u32[]{:S(2)}) copy-start(bf16[1,2048,256]{2,1,0:T(8,128)(2,1)} %param.25) | copy-start | bytes 3145732
  141.0 150.6 %reduce-scatter.5.cloned.1.call-start = ((), (), s32[]{:S(2)}) async-start(), calls=%async_computation.6 | async-start | bytes 10485760 | tf_op jit(solution)/shard_map/reduce_scatter | solution.py:91
  200.5 7.2 %copy-start.10 = (bf16[1,2048,256]{2,1,0:T(8,128)(2,1)S(1)}, bf16[1,2048,256]{2,1,0:T(8,128)(2,1)}, u32[]{:S(2)}) copy-start(bf16[1,2048,256]{2,1,0:T(8,128)(2,1)} %param.26) | copy-start | bytes 3145732
  291.6 6.0 %copy-start.6 = (f32[512]{0:T(512)S(1)}, f32[512]{0:T(512)}, u32[]{:S(2)}) copy-start(f32[512]{0:T(512)} %param.23) | copy-start | bytes 6148
  291.6 6.0 %copy-start.7 = (f32[512]{0:T(512)S(1)}, f32[512]{0:T(512)}, u32[]{:S(2)}) copy-start(f32[512]{0:T(512)} %param.24) | copy-start | bytes 6148
  291.6 49.9 %all-to-all-start.2 = ((bf16[8,256,512]{2,1,0:T(8,128)(2,1)}), bf16[8,256,512]{2,1,0:T(8,128)(2,1)S(1)}, u32[]{:S(2)}, u32[]{:S(2)}) async-start(bf16[8,256,512]{2,1,0:T(8,128)(2,1)} %bitcast.91), calls=%async_computation.4 | async-start | bytes 4194304 | tf_op jit(solution)/shard_map/all_to_all | solution.py:95
  348.9 1.7 copy-start.2
  349.0 1.6 copy-start.3
Sparse Core Ops, SparseCore 0:
  29.7 31.3 reduce-scatter.2
  141.1 59.3 all-gather.2
  220.9 70.6 reduce-scatter.4
where the time goes:
time: 365 us; the launch traced here: 358 us
  waiting for transfers between devices  210 us (58%)
  blocking collectives  64.3 us (18%)
  matrix products  22.4 us (6%)
  local copies, waits for them, and re-layouts  21.5 us (6%)
  starting transfers between devices  16.5 us (5%)
  between operations  13.4 us (4%)
  other arithmetic  10.5 us (3%)
    reduce_scatter x1, waiting for transfers between devices, shards(): lax.psum_scatter(partial_value.astype(jnp.bfloat16), 'tp', scatter_dimens...  70.8 us
    all_gather x1, waiting for transfers between devices, shards(): gathered = lax.all_gather(received[:, None], 'tp', axis=1, tiled=True)  59.3 us
    all_to_all x1, blocking collectives, shards(): lax.all_to_all(outgoing.reshape(seq_devices, capacity, D), 'sp', split_ax...  51.3 us
    all_to_all x1, waiting for transfers between devices, shards(): lax.all_to_all(columns.reshape(seq_devices, tp_devices * capacity, col_co...  43.8 us
    reduce_scatter x1, waiting for transfers between devices, shards(): lax.psum_scatter(partial_out.astype(jnp.bfloat16), 'tp', scatter_dimensio...  28 us
    dot_general x1, matrix products, shards(): jnp.dot(hidden, w_down[0], preferred_element_type=jnp.float32)  13.1 us
    all_to_all x1, waiting for transfers between devices, shards(): lax.all_to_all(normed, 'tp', split_axis=0, concat_axis=1, tiled=True)  7.52 us
  transfers between devices with their start and end apart: 7, of which 6 were waited for; matrix products, arithmetic and copies ran while one was open for 2% of the time, Pallas kernels for 0%

commit v1 on v0

v1 whole, which is shorter than its diff:
```python
import functools
import jax
import jax.numpy as jnp
from jax import lax
from jax.experimental import pallas as pl
from jax.experimental.pallas import tpu as pltpu
from jax.sharding import PartitionSpec as P

eps = 1e-06


def passed_along(value, axis, steps):
    count = lax.axis_size(axis)
    leading, last = (max(0, -steps), min(count, count - steps))
    return lax.ppermute(value, axis, [(source, source + steps) for source in range(leading, last)])


def sigmoid(v):
    return 1.0 / (1.0 + jnp.exp(-v))


def mix_kernel(rows, conv_ref, res_ref, weight_ref, slots_ref, middle_ref, out_ref):
    blocks, _, width = conv_ref.shape
    channels = blocks * width
    columns = res_ref.shape[2]
    features = blocks * columns
    total = jnp.zeros((rows, 1), jnp.float32)
    squares = jnp.zeros((rows, 1), jnp.float32)
    for b in range(blocks):
        part = conv_ref[b, :rows, :]
        total = total + jnp.sum(part, axis=-1, keepdims=True)
        squares = squares + jnp.sum(part * part, axis=-1, keepdims=True)
    mean = total / channels
    scale = lax.rsqrt(squares / channels - mean * mean + eps)
    mixed = jnp.zeros((rows, features), jnp.float32)
    for b in range(blocks):
        gain = conv_ref[b, rows : rows + 1, :]
        shift = conv_ref[b, rows + 1 : rows + 2, :]
        normalized = (conv_ref[b, :rows, :] - mean) * scale * gain + shift
        activated = (normalized * sigmoid(normalized)).astype(jnp.bfloat16)
        term = jnp.dot(activated, weight_ref[b], preferred_element_type=jnp.float32)
        mixed = mixed + term
    row_sq = jnp.zeros((rows, 1), jnp.float32)
    for b in range(blocks):
        span = slice(b * columns, (b + 1) * columns)
        middle = (res_ref[b].astype(jnp.float32) + mixed[:, span]).astype(jnp.bfloat16)
        middle_ref[b] = middle
        wide = middle.astype(jnp.float32)
        row_sq = row_sq + jnp.sum(wide * wide, axis=-1, keepdims=True)
    scale = lax.rsqrt(row_sq / features + eps)
    slot_num = out_ref.shape[0]
    at = lax.broadcasted_iota(jnp.int32, (slot_num, rows), 0)
    place = jnp.where((at == slots_ref[0:1, :]) | (at == slots_ref[1:2, :]), 1.0, 0.0).astype(jnp.bfloat16)
    pieces = columns // width
    for b in range(blocks):
        gains = [conv_ref[b, rows + 2 + i : rows + 3 + i, :] for i in range(pieces)]
        for i in range(pieces):
            wide = middle_ref[b, :, i * width : (i + 1) * width].astype(jnp.float32)
            normed = (wide * scale * gains[i]).astype(jnp.bfloat16)
            low = b * columns + i * width
            out_ref[:, low : low + width] = jnp.dot(
                place, normed, preferred_element_type=jnp.float32
            ).astype(jnp.bfloat16)


def mix(conv, residual, weight, slots, slot_num):
    blocks, rows, columns = residual.shape
    return pl.pallas_call(
        functools.partial(mix_kernel, rows),
        out_shape=(
            jax.ShapeDtypeStruct(residual.shape, jnp.bfloat16),
            jax.ShapeDtypeStruct((slot_num, blocks * columns), jnp.bfloat16),
        ),
        in_specs=[pl.BlockSpec(memory_space=pltpu.VMEM)] * 4,
        out_specs=[pl.BlockSpec(memory_space=pltpu.VMEM)] * 2,
        cost_estimate=pl.CostEstimate(
            flops=2 * rows * weight.size + 2 * slot_num * rows * blocks * columns,
            bytes_accessed=2 * weight.size + 4 * conv.size,
            transcendentals=0,
        ),
    )(conv, residual, weight, slots)


def expert_kernel(x_ref, gate_ref, up_ref, down_ref, out_ref, total):
    step = pl.program_id(0)

    @pl.when(step == 0)
    def _():
        total[...] = jnp.zeros_like(total)

    x = x_ref[...]
    gate = jnp.dot(x, gate_ref[0], preferred_element_type=jnp.float32)
    up = jnp.dot(x, up_ref[0], preferred_element_type=jnp.float32)
    hidden = (gate * sigmoid(gate) * up).astype(jnp.bfloat16)
    total[...] += jnp.dot(hidden, down_ref[0], preferred_element_type=jnp.float32)

    @pl.when(step == pl.num_programs(0) - 1)
    def _():
        out_ref[...] = total[...].astype(jnp.bfloat16)


def expert(x, w_gate, w_up, w_down):
    rows, features = x.shape
    blocks, _, width = w_gate.shape
    return pl.pallas_call(
        expert_kernel,
        grid=(blocks,),
        out_shape=jax.ShapeDtypeStruct((rows, features), jnp.bfloat16),
        in_specs=[
            pl.BlockSpec((rows, features), lambda b: (0, 0)),
            pl.BlockSpec((1, features, width), lambda b: (b, 0, 0)),
            pl.BlockSpec((1, features, width), lambda b: (b, 0, 0)),
            pl.BlockSpec((1, width, features), lambda b: (b, 0, 0)),
        ],
        out_specs=pl.BlockSpec((rows, features), lambda b: (0, 0)),
        scratch_shapes=[pltpu.VMEM((rows, features), jnp.float32)],
        cost_estimate=pl.CostEstimate(
            flops=6 * rows * w_gate.size,
            bytes_accessed=6 * w_gate.size + 4 * rows * features,
            transcendentals=rows * blocks * width,
        ),
    )(x, w_gate, w_up, w_down)


def combine_kernel(back_ref, middle_ref, slots_ref, gates_ref, out_ref):
    blocks, rows, columns = middle_ref.shape
    slot_num = back_ref.shape[0]
    at = lax.broadcasted_iota(jnp.int32, (rows, slot_num), 1)
    picks = [
        jnp.where(at == slots_ref[:, k : k + 1], 1.0, 0.0).astype(jnp.bfloat16) for k in range(2)
    ]
    weight, gap = gates_ref[:, 0:1], gates_ref[:, 1:2]
    gates = [weight * sigmoid(gap), weight * sigmoid(-gap)]
    for b in range(blocks):
        part = back_ref[:, b * columns : (b + 1) * columns]
        total = middle_ref[b].astype(jnp.float32)
        for k in range(2):
            total = total + gates[k] * jnp.dot(picks[k], part, preferred_element_type=jnp.float32)
        out_ref[b] = total.astype(jnp.bfloat16)


def combine(back, middle, slots, gates):
    return pl.pallas_call(
        combine_kernel,
        out_shape=jax.ShapeDtypeStruct(middle.shape, jnp.bfloat16),
        in_specs=[pl.BlockSpec(memory_space=pltpu.VMEM)] * 4,
        out_specs=pl.BlockSpec(memory_space=pltpu.VMEM),
        cost_estimate=pl.CostEstimate(
            flops=4 * middle.size * back.shape[0], bytes_accessed=2 * back.size, transcendentals=0
        ),
    )(back, middle, slots, gates)


def shards(
    conv_value,
    conv_gate,
    conv_weight,
    conv_gain,
    conv_shift,
    out_weight,
    residual,
    mix_gain,
    expert_ids,
    group_weight,
    score_gap,
    w_gate,
    w_up,
    w_down,
):
    row_count, width = conv_value.shape
    columns = residual.shape[1]
    reach_rows = conv_weight.shape[0] - 1
    seq_devices = lax.axis_size("sp")
    tp_devices = lax.axis_size("tp")
    quarter = row_count // tp_devices
    capacity = 4 * quarter // seq_devices
    slot_num = seq_devices * capacity
    my_index = lax.axis_index("tp")

    out_all = lax.all_gather(out_weight, "tp", axis=0, tiled=False)
    w_gate, w_up, w_down, _ = lax.optimization_barrier((w_gate[0], w_up[0], w_down[0], out_weight))
    gate_all = lax.all_gather(w_gate, "tp", axis=0, tiled=False)
    up_all = lax.all_gather(w_up, "tp", axis=0, tiled=False)
    down_all = lax.all_gather(w_down, "tp", axis=0, tiled=False)

    tails = jnp.concatenate(
        [conv_value[row_count - reach_rows :], conv_gate[row_count - reach_rows :]], axis=1
    )
    previous = passed_along(tails, "sp", 1)
    res_rows = lax.all_to_all(
        residual.reshape(tp_devices, quarter, columns), "tp", split_axis=0, concat_axis=0, tiled=True
    )
    values = jnp.concatenate([previous[:, :width], conv_value], axis=0).astype(jnp.float32)
    gate_pre = jnp.concatenate([previous[:, width:], conv_gate], axis=0).astype(jnp.float32)
    gated = values * jax.nn.sigmoid(gate_pre)
    convolved = jnp.zeros((row_count, width), jnp.float32)
    for tap_index in range(reach_rows + 1):
        convolved = convolved + conv_weight[tap_index] * gated[tap_index : tap_index + row_count]
    extras = jnp.concatenate(
        [conv_gain[None], conv_shift[None], mix_gain.reshape(-1, width)], axis=0
    )
    extras = jnp.pad(extras, ((0, -extras.shape[0] % 8), (0, 0)))
    message = jnp.concatenate(
        [
            convolved.reshape(tp_devices, quarter, width),
            jnp.broadcast_to(extras[None], (tp_devices,) + extras.shape),
        ],
        axis=1,
    )
    conv_rows = lax.all_to_all(message, "tp", split_axis=0, concat_axis=0, tiled=True)

    own = lax.dynamic_slice_in_dim(expert_ids, my_index * quarter, quarter, 0)
    flat = own.reshape(-1)
    onehot = (flat[:, None] == jnp.arange(seq_devices, dtype=jnp.int32)[None, :]).astype(jnp.bfloat16)
    order = jnp.arange(quarter * 2)
    lower = (order[:, None] > order[None, :]).astype(jnp.bfloat16)
    before = jnp.dot(lower, onehot, preferred_element_type=jnp.float32)
    rank = jnp.sum(before * onehot.astype(jnp.float32), axis=-1).astype(jnp.int32)
    slots = (flat * capacity + rank).reshape(quarter, 2)

    middle, outgoing = mix(conv_rows, res_rows, out_all, slots.T, slot_num)
    received = lax.all_to_all(
        outgoing.reshape(seq_devices, capacity, -1), "sp", split_axis=0, concat_axis=0, tiled=True
    )
    outputs = expert(received.reshape(slot_num, -1), gate_all, up_all, down_all)
    returned = lax.all_to_all(
        outputs.reshape(seq_devices, capacity, -1), "sp", split_axis=0, concat_axis=0, tiled=True
    )
    gates = jnp.stack([group_weight, score_gap], axis=1)
    own_gates = lax.dynamic_slice_in_dim(gates, my_index * quarter, quarter, 0)
    result = combine(returned.reshape(slot_num, -1), middle, slots, own_gates)
    result = lax.all_to_all(result, "tp", split_axis=0, concat_axis=0, tiled=True)
    return result.reshape(row_count, columns)


def solution(mesh):
    return jax.shard_map(
        shards,
        mesh=mesh,
        in_specs=(
            P("sp", "tp"),
            P("sp", "tp"),
            P(None, "tp"),
            P("tp"),
            P("tp"),
            P("tp", None),
            P("sp", "tp"),
            P("tp"),
            P("sp", None),
            P("sp"),
            P("sp"),
            P("sp", None, "tp"),
            P("sp", None, "tp"),
            P("sp", "tp", None),
        ),
        out_specs=P("sp", "tp"),
        check_vma=False,
    )
```

time: 365 us -> 256 us (0.70)
  the two profiles are of different devices: /device:TPU:17 before, /device:TPU:0 now
where the time goes in v1:
time: 256 us
  waiting for transfers between devices  178 us (70%)
  starting transfers between devices  22.5 us (9%)
  Pallas kernels  20.9 us (8%)
  between operations  13.4 us (5%)
  blocking collectives  12.3 us (5%)
  local copies, waits for them, and re-layouts  5.36 us (2%)
  other arithmetic  3.26 us (1%)
    all_to_all x1, waiting for transfers between devices, shards(): lax.all_to_all(outputs.reshape(seq_devices, capacity, -1), 'sp', split_ax...  47.8 us
    all_gather x1, waiting for transfers between devices, shards(): up_all = lax.all_gather(w_up, 'tp', axis=0, tiled=False)  36.1 us
    all_gather x1, waiting for transfers between devices, shards(): down_all = lax.all_gather(w_down, 'tp', axis=0, tiled=False)  35.9 us
    all_gather x1, waiting for transfers between devices, shards(): gate_all = lax.all_gather(w_gate, 'tp', axis=0, tiled=False)  24.9 us
    all_to_all x1, waiting for transfers between devices, shards(): lax.all_to_all(message, 'tp', split_axis=0, concat_axis=0, tiled=True)  14.2 us
    all_to_all x1, blocking collectives, shards(): lax.all_to_all(result, 'tp', split_axis=0, concat_axis=0, tiled=True)  12.3 us
    pallas_call x1, Pallas kernels, expert(): pl.pallas_call(expert_kernel, grid=(blocks,), out_shape=jax.ShapeDtypeStr...  12 us
    all_to_all x1, waiting for transfers between devices, shards(): lax.all_to_all(residual.reshape(tp_devices, quarter, columns), 'tp', spli...  10.5 us
  transfers between devices with their start and end apart: 9, of which 7 were waited for; matrix products, arithmetic and copies ran while one was open for 2% of the time, Pallas kernels for 2%

profile of v1, /device:TPU:0, one launch (start us, length us, event | category | flops | bytes accessed | tf_op | source)
XLA Modules:
  0.0 255.9 jit_solution(12518275284504465810)
XLA Ops:
  6.6 0.7 all-gather.9.cloned.1.call-update
  7.3 0.7 all-gather.11.cloned.1.call-update
  9.4 4.9 %collective-permute-start = (bf16[30,512]{1,0:T(8,128)(2,1)S(1)}, bf16[30,512]{1,0:T(8,128)(2,1)S(1)}, u32[]{:S(2)}, u32[]{:S(2)}) collective-permute-start(bf16[30,512]{1,0:T(8,128)(2,1)S(1)} %pad_maximum_fusion.1), channel_id=1, source_target_pairs={{0,4},{4,8},{8,12},{12,16},{16,20},{20,24},{24,28},{1,5},{5,9},{9,... | collective-permute-start | bytes 92168 | tf_op jit(solution)/shard_map/ppermute | solution.py:15
  14.3 3.5 %all-to-all-start.1 = ((bf16[4,128,512]{2,1,0:T(8,128)(2,1)}), bf16[4,128,512]{2,1,0:T(8,128)(2,1)S(1)}, u32[]{:S(2)}, u32[]{:S(2)}) async-start(bf16[4,128,512]{2,1,0:T(8,128)(2,1)} %bitcast.34), calls=%async_computation.1 | async-start | bytes 1048576 | tf_op jit(solution)/shard_map/all_to_all | solution.py:190
  18.2 2.1 fusion.1
  20.3 0.8 pad_maximum_fusion
  21.1 10.5 %all-to-all-done.1.res_ref = bf16[4,128,512]{2,1,0:T(8,128)(2,1)S(1)} async-done(((bf16[4,128,512]{2,1,0:T(8,128)(2,1)}), bf16[4,128,512]{2,1,0:T(8,128)(2,1)S(1)}, u32[]{:S(2)}, u32[]{:S(2)}) %all-to-all-start.1) | async-done | bytes 524320 | tf_op jit(solution)/shard_map/all_to_all | solution.py:190
  31.6 3.5 %all-to-all-start = ((f32[4,136,256]{2,1,0:T(8,128)}), f32[4,136,256]{2,1,0:T(8,128)S(1)}, u32[]{:S(2)}, u32[]{:S(2)}) async-start(f32[4,136,256]{2,1,0:T(8,128)} %pad_maximum_fusion), calls=%async_computation | async-start | bytes 1114112 | tf_op jit(solution)/shard_map/all_to_all | solution.py:210
  36.4 14.2 %all-to-all-done.conv_ref = f32[4,136,256]{2,1,0:T(8,128)S(1)} async-done(((f32[4,136,256]{2,1,0:T(8,128)}), f32[4,136,256]{2,1,0:T(8,128)S(1)}, u32[]{:S(2)}, u32[]{:S(2)}) %all-to-all-start) | async-done | bytes 557088 | tf_op jit(solution)/shard_map/all_to_all | solution.py:210
  50.6 6.0 %all-gather.9.cloned.1.call-done = bf16[1024,2048]{1,0:T(8,128)(2,1)} async-done(((bf16[256,2048]{1,0:T(8,128)(2,1)}), bf16[1024,2048]{1,0:T(8,128)(2,1)}) %all-gather.9.cloned.1.call-update) | async-done | bytes 4194320 | tf_op jit(solution)/shard_map/all_gather | solution.py:180
  56.6 5.6 %shard_map.136 = (bf16[4,128,512]{2,1,0:T(8,128)(2,1)}, bf16[512,2048]{1,0:T(8,128)(2,1)}) custom-call(f32[4,136,256]{2,1,0:T(8,128)} %copy-done.2, bf16[4,128,512]{2,1,0:T(8,128)(2,1)} %copy-done.3, bf16[4,256,2048]{2,1,0:T(8,128)(2,1)} %bitcast.51, s32[2,128]{1,0:T(2,128)} %copy.22.slots_ref), custom_call_target="tpu_custom_call" | custom-call | flops 805306368 | bytes 4751360 | tf_op jit(solution)/shard_map/pallas_call | solution.py:68
  62.3 4.9 %all-to-all-start.2 = ((bf16[8,64,2048]{2,1,0:T(8,128)(2,1)}), bf16[8,64,2048]{2,1,0:T(8,128)(2,1)S(1)}, u32[]{:S(2)}, u32[]{:S(2)}) async-start(bf16[8,64,2048]{2,1,0:T(8,128)(2,1)} %bitcast.54), calls=%async_computation.2 | async-start | bytes 4194304 | tf_op jit(solution)/shard_map/all_to_all | solution.py:222
  67.2 24.9 %all-gather.11.cloned.1.call-done = bf16[8192,256]{1,0:T(8,128)(2,1)} async-done(((bf16[2048,256]{1,0:T(8,128)(2,1)}), bf16[8192,256]{1,0:T(8,128)(2,1)}) %all-gather.11.cloned.1.call-update) | async-done | bytes 4194320 | tf_op jit(solution)/shard_map/all_gather | solution.py:182
  92.1 36.1 %all-gather.13.cloned.1.call-done = bf16[8192,256]{1,0:T(8,128)(2,1)} async-done(((bf16[2048,256]{1,0:T(8,128)(2,1)}), bf16[8192,256]{1,0:T(8,128)(2,1)}) %all-gather.13.cloned.1.call-update) | async-done | bytes 4194320 | tf_op jit(solution)/shard_map/all_gather | solution.py:183
  128.1 35.9 %all-gather.15.cloned.1.call-done = bf16[1024,2048]{1,0:T(8,128)(2,1)} async-done(((bf16[256,2048]{1,0:T(8,128)(2,1)}), bf16[1024,2048]{1,0:T(8,128)(2,1)}) %all-gather.15.cloned.1.call-update) | async-done | bytes 4194320 | tf_op jit(solution)/shard_map/all_gather | solution.py:184
  164.0 1.3 copy-done.4
  165.3 12.0 %shard_map.137 = bf16[512,2048]{1,0:T(8,128)(2,1)} custom-call(bf16[512,2048]{1,0:T(8,128)(2,1)} %bitcast.53, bf16[4,2048,256]{2,1,0:T(8,128)(2,1)} %bitcast.96, bf16[4,2048,256]{2,1,0:T(8,128)(2,1)} %bitcast.97, bf16[4,256,2048]{2,1,0:T(8,128)(2,1)} %bitcast.98), custom_call_target="tpu_custom_call" | custom-call | flops 6442450944 | bytes 16777216 | tf_op jit(solution)/shard_map/pallas_call | solution.py:105
  177.3 5.6 %all-to-all-start.3 = ((bf16[8,64,2048]{2,1,0:T(8,128)(2,1)}), bf16[8,64,2048]{2,1,0:T(8,128)(2,1)S(1)}, u32[]{:S(2)}, u32[]{:S(2)}) async-start(bf16[8,64,2048]{2,1,0:T(8,128)(2,1)} %bitcast.55), calls=%async_computation.3 | async-start | bytes 4194304 | tf_op jit(solution)/shard_map/all_to_all | solution.py:226
  183.0 0.7 copy.25.gates_ref
  183.8 47.8 %all-to-all-done.3 = bf16[8,64,2048]{2,1,0:T(8,128)(2,1)S(1)} async-done(((bf16[8,64,2048]{2,1,0:T(8,128)(2,1)}), bf16[8,64,2048]{2,1,0:T(8,128)(2,1)S(1)}, u32[]{:S(2)}, u32[]{:S(2)}) %all-to-all-start.3) | async-done | bytes 2097184 | tf_op jit(solution)/shard_map/all_to_all | solution.py:226
  231.6 1.3 copy-done.1
  232.9 3.4 %shard_map.138 = bf16[4,128,512]{2,1,0:T(8,128)(2,1)} custom-call(bf16[512,2048]{1,0:T(8,128)(2,1)} %bitcast.50, bf16[4,128,512]{2,1,0:T(8,128)(2,1)} %get-tuple-element.14.middle_ref, s32[128,2]{1,0:T(8,128)} %copy-done.5, f32[128,2]{1,0:T(8,128)} %copy.25.gates_ref), custom_call_target="tpu_custom_call" | custom-call | flops 536870912 | bytes 2097152 | tf_op jit(solution)/shard_map/pallas_call | solution.py:143
  236.3 12.3 %all_to_all.25 = bf16[4,128,512]{2,1,0:T(8,128)(2,1)S(1)} all-to-all(bf16[4,128,512]{2,1,0:T(8,128)(2,1)} %shard_map.138), channel_id=1, replica_groups=mesh['sp'=8,'tp'=4] {'tp'}, dimensions={0} | all-to-all | bytes 1048576 | tf_op jit(solution)/shard_map/all_to_all | solution.py:232
  248.5 0.8 copy.27
  (53 shorter events, 3.1 us)
Async XLA Ops:
  6.5 28.6 %copy-start = (s32[512,2]{0,1:T(2,128)S(1)}, s32[512,2]{0,1:T(2,128)}, u32[]{:S(2)}) copy-start(s32[512,2]{0,1:T(2,128)} %param.22) | copy-start | bytes 12292
  6.5 2.8 %copy-start.6 = (bf16[512,256]{1,0:T(8,128)(2,1)S(1)}, bf16[512,256]{1,0:T(8,128)(2,1)}, u32[]{:S(2)}) copy-start(bf16[512,256]{1,0:T(8,128)(2,1)} %param.14) | copy-start | bytes 786436
  6.5 2.9 %copy-start.7 = (bf16[512,256]{1,0:T(8,128)(2,1)S(1)}, bf16[512,256]{1,0:T(8,128)(2,1)}, u32[]{:S(2)}) copy-start(bf16[512,256]{1,0:T(8,128)(2,1)} %param.15) | copy-start | bytes 786436
  6.5 11.3 %copy-start.9 = (f32[512]{0:T(512)S(1)}, f32[512]{0:T(512)}, u32[]{:S(2)}) copy-start(f32[512]{0:T(512)} %param.21) | copy-start | bytes 6148
  6.5 11.3 %copy-start.8 = (f32[31,256]{1,0:T(8,128)S(1)}, f32[31,256]{1,0:T(8,128)}, u32[]{:S(2)}) copy-start(f32[31,256]{1,0:T(8,128)} %param.16) | copy-start | bytes 95236
  6.5 11.3 %copy-start.13 = (f32[256]{0:T(256)S(1)}, f32[256]{0:T(256)}, u32[]{:S(2)}) copy-start(f32[256]{0:T(256)} %param.17) | copy-start | bytes 3076
  6.6 11.3 %copy-start.12 = (f32[256]{0:T(256)S(1)}, f32[256]{0:T(256)}, u32[]{:S(2)}) copy-start(f32[256]{0:T(256)} %param.18) | copy-start | bytes 3076
  6.6 50.1 %all-gather.9.cloned.1.call-start = ((), (), s32[]{:S(2)}) async-start(), calls=%async_computation.5 | async-start | bytes 5242880 | tf_op jit(solution)/shard_map/all_gather | solution.py:180
  7.3 84.8 %all-gather.11.cloned.1.call-start = ((), (), s32[]{:S(2)}) async-start(), calls=%async_computation.6 | async-start | bytes 5242880 | tf_op jit(solution)/shard_map/all_gather | solution.py:182
  8.1 120.1 %all-gather.13.cloned.1.call-start = ((), (), s32[]{:S(2)}) async-start(), calls=%async_computation.7 | async-start | bytes 5242880 | tf_op jit(solution)/shard_map/all_gather | solution.py:183
  8.8 155.2 %all-gather.15.cloned.1.call-start = ((), (), s32[]{:S(2)}) async-start(), calls=%async_computation.8 | async-start | bytes 5242880 | tf_op jit(solution)/shard_map/all_gather | solution.py:184
  9.4 8.5 %collective-permute-start = (bf16[30,512]{1,0:T(8,128)(2,1)S(1)}, bf16[30,512]{1,0:T(8,128)(2,1)S(1)}, u32[]{:S(2)}, u32[]{:S(2)}) collective-permute-start(bf16[30,512]{1,0:T(8,128)(2,1)S(1)} %pad_maximum_fusion.1), channel_id=1, source_target_pairs={{0,4},{4,8},{8,12},{12,16},{16,20},{20,24},{24,28},{1,5},{5,9},{9,... | collective-permute-start | bytes 92168 | tf_op jit(solution)/shard_map/ppermute | solution.py:15
  14.3 17.3 %all-to-all-start.1 = ((bf16[4,128,512]{2,1,0:T(8,128)(2,1)}), bf16[4,128,512]{2,1,0:T(8,128)(2,1)S(1)}, u32[]{:S(2)}, u32[]{:S(2)}) async-start(bf16[4,128,512]{2,1,0:T(8,128)(2,1)} %bitcast.34), calls=%async_computation.1 | async-start | bytes 1048576 | tf_op jit(solution)/shard_map/all_to_all | solution.py:190
  31.6 25.0 %copy-start.3 = (bf16[4,128,512]{2,1,0:T(8,128)(2,1)}, bf16[4,128,512]{2,1,0:T(8,128)(2,1)S(1)}, u32[]{:S(2)}) copy-start(bf16[4,128,512]{2,1,0:T(8,128)(2,1)S(1)} %all-to-all-done.1.res_ref) | copy-start | bytes 1572868
  31.6 19.0 %all-to-all-start = ((f32[4,136,256]{2,1,0:T(8,128)}), f32[4,136,256]{2,1,0:T(8,128)S(1)}, u32[]{:S(2)}, u32[]{:S(2)}) async-start(f32[4,136,256]{2,1,0:T(8,128)} %pad_maximum_fusion), calls=%async_computation | async-start | bytes 1114112 | tf_op jit(solution)/shard_map/all_to_all | solution.py:210
  35.8 26.5 %copy-start.5 = (s32[128,2]{1,0:T(8,128)}, s32[128,2]{1,0:T(8,128)S(1)}, u32[]{:S(2)}) copy-start(s32[128,2]{1,0:T(8,128)S(1)} %multiply_add_fusion.slots_ref) | copy-start | bytes 3076
  50.6 6.0 %copy-start.2 = (f32[4,136,256]{2,1,0:T(8,128)}, f32[4,136,256]{2,1,0:T(8,128)S(1)}, u32[]{:S(2)}) copy-start(f32[4,136,256]{2,1,0:T(8,128)S(1)} %all-to-all-done.conv_ref) | copy-start | bytes 1671172
  62.3 101.8 %all-to-all-start.2 = ((bf16[8,64,2048]{2,1,0:T(8,128)(2,1)}), bf16[8,64,2048]{2,1,0:T(8,128)(2,1)S(1)}, u32[]{:S(2)}, u32[]{:S(2)}) async-start(bf16[8,64,2048]{2,1,0:T(8,128)(2,1)} %bitcast.54), calls=%async_computation.2 | async-start | bytes 4194304 | tf_op jit(solution)/shard_map/all_to_all | solution.py:222
  164.0 1.3 copy-start.4
  177.3 5.6 %copy-start.10 = (f32[512]{0:T(512)S(1)}, f32[512]{0:T(512)}, u32[]{:S(2)}) copy-start(f32[512]{0:T(512)} %param.23) | copy-start | bytes 6148
  177.3 5.7 %copy-start.11 = (f32[512]{0:T(512)S(1)}, f32[512]{0:T(512)}, u32[]{:S(2)}) copy-start(f32[512]{0:T(512)} %param.24) | copy-start | bytes 6148
  177.3 54.3 %all-to-all-start.3 = ((bf16[8,64,2048]{2,1,0:T(8,128)(2,1)}), bf16[8,64,2048]{2,1,0:T(8,128)(2,1)S(1)}, u32[]{:S(2)}, u32[]{:S(2)}) async-start(bf16[8,64,2048]{2,1,0:T(8,128)(2,1)} %bitcast.55), calls=%async_computation.3 | async-start | bytes 4194304 | tf_op jit(solution)/shard_map/all_to_all | solution.py:226
  231.6 1.3 copy-start.1
Sparse Core Ops, SparseCore 0:
  8.9 47.6 all-gather.8
  58.2 33.8 all-gather.10
  93.6 34.4 all-gather.12
  129.5 34.4 all-gather.14

commit v2 on v1

--- a/solution.py
+++ b/solution.py
@@ -81,74 +81,215 @@
     )(conv, residual, weight, slots)
 
 
-def expert_kernel(x_ref, gate_ref, up_ref, down_ref, out_ref, total):
-    step = pl.program_id(0)
-
-    @pl.when(step == 0)
-    def _():
-        total[...] = jnp.zeros_like(total)
-
-    x = x_ref[...]
-    gate = jnp.dot(x, gate_ref[0], preferred_element_type=jnp.float32)
-    up = jnp.dot(x, up_ref[0], preferred_element_type=jnp.float32)
-    hidden = (gate * sigmoid(gate) * up).astype(jnp.bfloat16)
-    total[...] += jnp.dot(hidden, down_ref[0], preferred_element_type=jnp.float32)
-
-    @pl.when(step == pl.num_programs(0) - 1)
-    def _():
-        out_ref[...] = total[...].astype(jnp.bfloat16)
-
-
-def expert(x, w_gate, w_up, w_down):
-    rows, features = x.shape
-    blocks, _, width = w_gate.shape
-    return pl.pallas_call(
-        expert_kernel,
-        grid=(blocks,),
-        out_shape=jax.ShapeDtypeStruct((rows, features), jnp.bfloat16),
-        in_specs=[
-            pl.BlockSpec((rows, features), lambda b: (0, 0)),
-            pl.BlockSpec((1, features, width), lambda b: (b, 0, 0)),
-            pl.BlockSpec((1, features, width), lambda b: (b, 0, 0)),
-            pl.BlockSpec((1, width, features), lambda b: (b, 0, 0)),
-        ],
-        out_specs=pl.BlockSpec((rows, features), lambda b: (0, 0)),
-        scratch_shapes=[pltpu.VMEM((rows, features), jnp.float32)],
-        cost_estimate=pl.CostEstimate(
-            flops=6 * rows * w_gate.size,
-            bytes_accessed=6 * w_gate.size + 4 * rows * features,
-            transcendentals=rows * blocks * width,
-        ),
-    )(x, w_gate, w_up, w_down)
-
-
-def combine_kernel(back_ref, middle_ref, slots_ref, gates_ref, out_ref):
+def expert_kernel(
+    seq_num,
+    x_ref,
+    gate_ref,
+    up_ref,
+    down_ref,
+    middle_ref,
+    slots_ref,
+    gates_ref,
+    out_ref,
+    received,
+    gate_all,
+    up_all,
+    down_all,
+    total,
+    outputs,
+    back,
+    result,
+    final,
+    x_send,
+    x_recv,
+    w_send,
+    w_recv,
+    y_send,
+    y_recv,
+    r_send,
+    r_recv,
+    own_sem,
+):
     blocks, rows, columns = middle_ref.shape
-    slot_num = back_ref.shape[0]
-    at = lax.broadcasted_iota(jnp.int32, (rows, slot_num), 1)
+    slot_num = x_ref.shape[0]
+    capacity = slot_num // seq_num
+    me, mine = lax.axis_index("sp"), lax.axis_index("tp")
+    partner = mine + 1 - 2 * lax.rem(mine, 2)
+    counter = lax.rem(mine + blocks // 2, blocks)
+    diagonal = lax.rem(partner + blocks // 2, blocks)
+    mates = (partner, counter, diagonal)
+    steps = sorted(range(1, seq_num), key=lambda i: abs(2 * i - seq_num))
+
+    def to_seq(i):
+        return {"sp": lax.rem(me + i, seq_num)}
+
+    barrier = pltpu.get_barrier_semaphore()
+    for mate in mates:
+        pl.semaphore_signal(barrier, inc=1, device_id={"tp": mate}, device_id_type=pl.DeviceIdType.MESH)
+    for i in steps:
+        pl.semaphore_signal(barrier, inc=1, device_id=to_seq(i), device_id_type=pl.DeviceIdType.MESH)
+    pl.semaphore_wait(barrier, len(mates) + len(steps))
+
+    def remote(src, dst, send, recv, device):
+        copy = pltpu.make_async_remote_copy(
+            src_ref=src,
+            dst_ref=dst,
+            send_sem=send,
+            recv_sem=recv,
+            device_id=device,
+            device_id_type=pl.DeviceIdType.MESH,
+        )
+        copy.start()
+        return copy
+
+    def at(index):
+        return pl.ds(pl.multiple_of(index * capacity, capacity), capacity)
+
+    weights = ((gate_ref, gate_all), (up_ref, up_all), (down_ref, down_all))
+    across, beside, own = [], [], []
+    for k, (source, held) in enumerate(weights):
+        across.append(
+            remote(source, held.at[2], w_send.at[k, 2], w_recv.at[k, 2], {"tp": counter})
+        )
+    x_copies = []
+    for i in steps:
+        peer = lax.rem(me + i, seq_num)
+        x_copies.append(
+            remote(x_ref.at[at(peer)], received.at[at(me)], x_send.at[i], x_recv.at[i], to_seq(i))
+        )
+    for k, (source, held) in enumerate(weights):
+        beside.append(
+            remote(source, held.at[1], w_send.at[k, 1], w_recv.at[k, 1], {"tp": partner})
+        )
+        copy = pltpu.make_async_copy(source, held.at[0], own_sem.at[k])
+        copy.start()
+        own.append(copy)
+    own_x = pltpu.make_async_copy(x_ref.at[at(me)], received.at[at(me)], own_sem.at[3])
+    own_x.start()
+
+    def forward(k):
+        held = weights[k][1]
+        across[k].wait_recv()
+        return remote(held.at[2], held.at[3], w_send.at[k, 3], w_recv.at[k, 3], {"tp": partner})
+
+    total[...] = jnp.zeros_like(total)
+    passed = [forward(0), forward(1)]
+    own_x.wait()
+    for copy in own:
+        copy.wait()
+    for copy in beside:
+        copy.wait_recv()
+    for copy in x_copies:
+        copy.wait_recv()
+    passed_down = pltpu.make_async_remote_copy(
+        src_ref=down_all.at[2],
+        dst_ref=down_all.at[3],
+        send_sem=w_send.at[2, 3],
+        recv_sem=w_recv.at[2, 3],
+        device_id={"tp": partner},
+        device_id_type=pl.DeviceIdType.MESH,
+    )
+
+    @pl.loop(0, blocks)
+    def _(b):
+        @pl.when(b == 2)
+        def _():
+            across[2].wait_recv()
+            passed_down.start()
+
+        @pl.when(b == 3)
+        def _():
+            for copy in passed:
+                copy.wait_recv()
+            passed_down.wait_recv()
+
+        x = received[...]
+        gate = jnp.dot(x, gate_all[b], preferred_element_type=jnp.float32)
+        up = jnp.dot(x, up_all[b], preferred_element_type=jnp.float32)
+        hidden = (gate * sigmoid(gate) * up).astype(jnp.bfloat16)
+        total[...] += jnp.dot(hidden, down_all[b], preferred_element_type=jnp.float32)
+
+    outputs[...] = total[...].astype(jnp.bfloat16)
+    y_copies = []
+    for i in steps:
+        peer = lax.rem(me + i, seq_num)
+        y_copies.append(
+            remote(outputs.at[at(peer)], back.at[at(me)], y_send.at[i], y_recv.at[i], to_seq(i))
+        )
+    own_y = pltpu.make_async_copy(outputs.at[at(me)], back.at[at(me)], own_sem.at[4])
+    own_y.start()
+    for copy in across + beside + passed + [passed_down] + x_copies:
+        copy.wait_send()
+    where = lax.broadcasted_iota(jnp.int32, (rows, slot_num), 1)
     picks = [
-        jnp.where(at == slots_ref[:, k : k + 1], 1.0, 0.0).astype(jnp.bfloat16) for k in range(2)
+        jnp.where(where == slots_ref[:, k : k + 1], 1.0, 0.0).astype(jnp.bfloat16) for k in range(2)
     ]
     weight, gap = gates_ref[:, 0:1], gates_ref[:, 1:2]
     gates = [weight * sigmoid(gap), weight * sigmoid(-gap)]
-    for b in range(blocks):
-        part = back_ref[:, b * columns : (b + 1) * columns]
-        total = middle_ref[b].astype(jnp.float32)
+    own_y.wait()
+    for copy in y_copies:
+        copy.wait_recv()
+    for b in range(blocks):
+        part = back[:, b * columns : (b + 1) * columns]
+        value = middle_ref[b].astype(jnp.float32)
         for k in range(2):
-            total = total + gates[k] * jnp.dot(picks[k], part, preferred_element_type=jnp.float32)
-        out_ref[b] = total.astype(jnp.bfloat16)
-
-
-def combine(back, middle, slots, gates):
+            value = value + gates[k] * jnp.dot(picks[k], part, preferred_element_type=jnp.float32)
+        result[b] = value.astype(jnp.bfloat16)
+    rows_at = pl.ds(pl.multiple_of(mine * rows, rows), rows)
+    r_copies = []
+    for j, mate in ((1, counter), (2, diagonal), (0, partner)):
+        r_copies.append(
+            remote(result.at[mate], final.at[rows_at], r_send.at[j], r_recv.at[j], {"tp": mate})
+        )
+    own_r = pltpu.make_async_copy(result.at[mine], final.at[rows_at], own_sem.at[5])
+    own_r.start()
+    for copy in y_copies:
+        copy.wait_send()
+    own_r.wait()
+    for copy in r_copies:
+        copy.wait()
+    out_ref[...] = final[...]
+
+
+def expert(x, w_gate, w_up, w_down, middle, slots, gates, seq_num):
+    slot_num, features = x.shape
+    blocks, rows, columns = middle.shape
+    width = w_gate.shape[1]
+    vmem, anywhere = pl.BlockSpec(memory_space=pltpu.VMEM), pl.BlockSpec(memory_space=pl.ANY)
+    wide = (slot_num, features)
+    dma = pltpu.SemaphoreType.DMA
     return pl.pallas_call(
-        combine_kernel,
-        out_shape=jax.ShapeDtypeStruct(middle.shape, jnp.bfloat16),
-        in_specs=[pl.BlockSpec(memory_space=pltpu.VMEM)] * 4,
-        out_specs=pl.BlockSpec(memory_space=pltpu.VMEM),
+        functools.partial(expert_kernel, seq_num),
+        out_shape=jax.ShapeDtypeStruct((blocks * rows, columns), jnp.bfloat16),
+        in_specs=[vmem, anywhere, anywhere, anywhere, vmem, vmem, vmem],
+        out_specs=vmem,
+        scratch_shapes=[
+            pltpu.VMEM(wide, jnp.bfloat16),
+            pltpu.VMEM((blocks, features, width), jnp.bfloat16),
+            pltpu.VMEM((blocks, features, width), jnp.bfloat16),
+            pltpu.VMEM((blocks, width, features), jnp.bfloat16),
+            pltpu.VMEM(wide, jnp.float32),
+            pltpu.VMEM(wide, jnp.bfloat16),
+            pltpu.VMEM(wide, jnp.bfloat16),
+            pltpu.VMEM(middle.shape, jnp.bfloat16),
+            pltpu.VMEM((blocks * rows, columns), jnp.bfloat16),
+            dma((seq_num,)),
+            dma((seq_num,)),
+            dma((3, blocks)),
+            dma((3, blocks)),
+            dma((seq_num,)),
+            dma((seq_num,)),
+            dma((blocks,)),
+            dma((blocks,)),
+            dma((6,)),
+        ],
+        compiler_params=pltpu.CompilerParams(collective_id=0, has_side_effects=True),
         cost_estimate=pl.CostEstimate(
-            flops=4 * middle.size * back.shape[0], bytes_accessed=2 * back.size, transcendentals=0
+            flops=6 * slot_num * w_gate.size * blocks,
+            bytes_accessed=6 * w_gate.size * blocks,
+            transcendentals=slot_num * blocks * width,
         ),
-    )(back, middle, slots, gates)
+    )(x, w_gate, w_up, w_down, middle, slots, gates)
 
 
 def shards(
@@ -178,10 +319,6 @@
     my_index = lax.axis_index("tp")
 
     out_all = lax.all_gather(out_weight, "tp", axis=0, tiled=False)
-    w_gate, w_up, w_down, _ = lax.optimization_barrier((w_gate[0], w_up[0], w_down[0], out_weight))
-    gate_all = lax.all_gather(w_gate, "tp", axis=0, tiled=False)
-    up_all = lax.all_gather(w_up, "tp", axis=0, tiled=False)
-    down_all = lax.all_gather(w_down, "tp", axis=0, tiled=False)
 
     tails = jnp.concatenate(
         [conv_value[row_count - reach_rows :], conv_gate[row_count - reach_rows :]], axis=1
@@ -219,18 +356,11 @@
     slots = (flat * capacity + rank).reshape(quarter, 2)
 
     middle, outgoing = mix(conv_rows, res_rows, out_all, slots.T, slot_num)
-    received = lax.all_to_all(
-        outgoing.reshape(seq_devices, capacity, -1), "sp", split_axis=0, concat_axis=0, tiled=True
-    )
-    outputs = expert(received.reshape(slot_num, -1), gate_all, up_all, down_all)
-    returned = lax.all_to_all(
-        outputs.reshape(seq_devices, capacity, -1), "sp", split_axis=0, concat_axis=0, tiled=True
-    )
     gates = jnp.stack([group_weight, score_gap], axis=1)
     own_gates = lax.dynamic_slice_in_dim(gates, my_index * quarter, quarter, 0)
-    result = combine(returned.reshape(slot_num, -1), middle, slots, own_gates)
-    result = lax.all_to_all(result, "tp", split_axis=0, concat_axis=0, tiled=True)
-    return result.reshape(row_count, columns)
+    return expert(
+        outgoing, w_gate[0], w_up[0], w_down[0], middle, slots, own_gates, seq_devices
+    )
 
 
 def solution(mesh):

time: 256 us -> 205 us (0.80)
  the two profiles are of different devices: /device:TPU:0 before, /device:TPU:17 now
where the time goes in v2:
time: 205 us; the launch traced here: 204 us
  Pallas kernels  140 us (68%)
  waiting for transfers between devices  24 us (12%)
  between operations  13.5 us (7%)
  starting transfers between devices  13 us (6%)
  local copies, waits for them, and re-layouts  7.83 us (4%)
  other arithmetic  5.04 us (2%)
    pallas_call x1, Pallas kernels, expert(): pl.pallas_call(functools.partial(expert_kernel, seq_num), out_shape=jax.S...  135 us
    all_to_all x1, waiting for transfers between devices, shards(): lax.all_to_all(message, 'tp', split_axis=0, concat_axis=0, tiled=True)  13 us
    all_gather x1, waiting for transfers between devices, shards(): out_all = lax.all_gather(out_weight, 'tp', axis=0, tiled=False)  6.96 us
    pallas_call x1, Pallas kernels, mix(): pl.pallas_call(functools.partial(mix_kernel, rows), out_shape=(jax.ShapeD...  5.63 us
    all_to_all x1, starting transfers between devices, shards(): lax.all_to_all(message, 'tp', split_axis=0, concat_axis=0, tiled=True)  5.45 us
    all_to_all x1, starting transfers between devices, shards(): lax.all_to_all(residual.reshape(tp_devices, quarter, columns), 'tp', spli...  4.41 us
  transfers between devices with their start and end apart: 4, of which 3 were waited for; matrix products, arithmetic and copies ran while one was open for 5% of the time, Pallas kernels for 0%

profile of v2, /device:TPU:17, one launch (start us, length us, event | category | flops | bytes accessed | tf_op | source)
XLA Modules:
  0.0 203.9 jit_solution(12747915666996492155)
XLA Ops:
  6.5 0.7 all-gather.3.cloned.1.call-update
  7.3 0.7 slice.199
  8.0 0.7 slice.200
  8.7 3.1 %collective-permute-start = (bf16[30,512]{1,0:T(8,128)(2,1)S(1)}, bf16[30,512]{1,0:T(8,128)(2,1)S(1)}, u32[]{:S(2)}, u32[]{:S(2)}) collective-permute-start(bf16[30,512]{1,0:T(8,128)(2,1)S(1)} %pad_maximum_fusion.1), channel_id=1, source_target_pairs={{0,4},{4,8},{8,12},{12,16},{16,20},{20,24},{24,28},{1,5},{5,9},{9,... | collective-permute-start | bytes 92168 | tf_op jit(solution)/shard_map/ppermute | solution.py:15
  11.8 4.4 %all-to-all-start.1 = ((bf16[4,128,512]{2,1,0:T(8,128)(2,1)}), bf16[4,128,512]{2,1,0:T(8,128)(2,1)S(1)}, u32[]{:S(2)}, u32[]{:S(2)}) async-start(bf16[4,128,512]{2,1,0:T(8,128)(2,1)} %bitcast.44), calls=%async_computation.1 | async-start | bytes 1048576 | tf_op jit(solution)/shard_map/all_to_all | solution.py:327
  16.3 0.7 reshape.16
  17.0 0.7 select_maximum_fusion
  17.7 1.0 fusion.35
  18.6 1.0 fusion.34
  19.8 0.1 eq.15
  20.0 1.3 divide_multiply_fusion
  21.3 2.1 %fusion.1 = f32[512,256]{1,0:T(8,128)S(1)} fusion(f32[542,256]{1,0:T(8,128)S(1)} %divide_multiply_fusion, f32[256]{0:T(256)S(1)} %bitcast.56, f32[256]{0:T(256)S(1)} %bitcast.57, f32[256]{0:T(256)S(1)} %bitcast.59, f32[256]{0:T(256)S(1)} %bitcast.60, f32[256]{0:T(256)S(1)} %bitcast.61, f32[256]{0:T(256)S(1)} %bitcast.62, f32[256]{0:T(256)S(1)} %bitcast.63, ...), kind=kLoop, calls=%fused_computation.5 | loop fusion | flops 7995392 | bytes 16808960 | tf_op jit(solution)/shard_map/add | solution.py:335
  23.4 0.9 pad_maximum_fusion
  24.2 3.4 %all-to-all-done.1.res_ref = bf16[4,128,512]{2,1,0:T(8,128)(2,1)S(1)} async-done(((bf16[4,128,512]{2,1,0:T(8,128)(2,1)}), bf16[4,128,512]{2,1,0:T(8,128)(2,1)S(1)}, u32[]{:S(2)}, u32[]{:S(2)}) %all-to-all-start.1) | async-done | bytes 524320 | tf_op jit(solution)/shard_map/all_to_all | solution.py:327
  27.6 5.5 %all-to-all-start = ((f32[4,136,256]{2,1,0:T(8,128)}), f32[4,136,256]{2,1,0:T(8,128)S(1)}, u32[]{:S(2)}, u32[]{:S(2)}) async-start(f32[4,136,256]{2,1,0:T(8,128)} %pad_maximum_fusion), calls=%async_computation | async-start | bytes 1114112 | tf_op jit(solution)/shard_map/all_to_all | solution.py:347
  33.1 0.2 fusion
  33.3 0.1 convert_element_type.27
  33.4 0.7 copy.22.slots_ref
  34.2 0.7 copy.25.gates_ref
  34.9 13.0 %all-to-all-done.conv_ref = f32[4,136,256]{2,1,0:T(8,128)S(1)} async-done(((f32[4,136,256]{2,1,0:T(8,128)}), f32[4,136,256]{2,1,0:T(8,128)S(1)}, u32[]{:S(2)}, u32[]{:S(2)}) %all-to-all-start) | async-done | bytes 557088 | tf_op jit(solution)/shard_map/all_to_all | solution.py:347
  47.9 7.0 %all-gather.3.cloned.1.call-done = bf16[1024,2048]{1,0:T(8,128)(2,1)} async-done(((bf16[256,2048]{1,0:T(8,128)(2,1)}), bf16[1024,2048]{1,0:T(8,128)(2,1)}) %all-gather.3.cloned.1.call-update) | async-done | bytes 4194320 | tf_op jit(solution)/shard_map/all_gather | solution.py:321
  54.9 5.6 %shard_map.136 = (bf16[4,128,512]{2,1,0:T(8,128)(2,1)}, bf16[512,2048]{1,0:T(8,128)(2,1)}) custom-call(f32[4,136,256]{2,1,0:T(8,128)} %copy-done.1, bf16[4,128,512]{2,1,0:T(8,128)(2,1)} %copy-done.2, bf16[4,256,2048]{2,1,0:T(8,128)(2,1)} %bitcast.42, s32[2,128]{1,0:T(2,128)} %copy.22.slots_ref), custom_call_target="tpu_custom_call" | custom-call | flops 805306368 | bytes 4751360 | tf_op jit(solution)/shard_map/pallas_call | solution.py:68
  60.5 134.7 %shard_map.137 = bf16[512,512]{1,0:T(8,128)(2,1)} custom-call(bf16[512,2048]{1,0:T(8,128)(2,1)} %get-tuple-element.7.x_ref, bf16[2048,256]{1,0:T(8,128)(2,1)} %bitcast.81, bf16[2048,256]{1,0:T(8,128)(2,1)} %bitcast.82, bf16[256,2048]{1,0:T(8,128)(2,1)} %bitcast.83, bf16[4,128,512]{2,1,0:T(8,128)(2,1)} %get-tuple-element.8.middle_ref, s32[128,2]{1,0:T(8,128)} %copy-done.3, ...), custom_call_target="tpu_custom_call" | custom-call | flops 6442450944 | bytes 12582912 | tf_op jit(solution)/shard_map/pallas_call | solution.py:261
  195.2 1.9 copy.27
  (22 shorter events, 0.3 us)
Async XLA Ops:
  6.5 13.1 %copy-start = (s32[512,2]{0,1:T(2,128)S(1)}, s32[512,2]{0,1:T(2,128)}, u32[]{:S(2)}) copy-start(s32[512,2]{0,1:T(2,128)} %param.22) | copy-start | bytes 12292
  6.5 48.3 %all-gather.3.cloned.1.call-start = ((), (), s32[]{:S(2)}) async-start(), calls=%async_computation.2 | async-start | bytes 5242880 | tf_op jit(solution)/shard_map/all_gather | solution.py:321
  8.7 11.2 %collective-permute-start = (bf16[30,512]{1,0:T(8,128)(2,1)S(1)}, bf16[30,512]{1,0:T(8,128)(2,1)S(1)}, u32[]{:S(2)}, u32[]{:S(2)}) collective-permute-start(bf16[30,512]{1,0:T(8,128)(2,1)S(1)} %pad_maximum_fusion.1), channel_id=1, source_target_pairs={{0,4},{4,8},{8,12},{12,16},{16,20},{20,24},{24,28},{1,5},{5,9},{9,... | collective-permute-start | bytes 92168 | tf_op jit(solution)/shard_map/ppermute | solution.py:15
  11.8 15.8 %all-to-all-start.1 = ((bf16[4,128,512]{2,1,0:T(8,128)(2,1)}), bf16[4,128,512]{2,1,0:T(8,128)(2,1)S(1)}, u32[]{:S(2)}, u32[]{:S(2)}) async-start(bf16[4,128,512]{2,1,0:T(8,128)(2,1)} %bitcast.44), calls=%async_computation.1 | async-start | bytes 1048576 | tf_op jit(solution)/shard_map/all_to_all | solution.py:327
  21.3 12.8 %copy-start.4 = (f32[512]{0:T(512)S(1)}, f32[512]{0:T(512)}, u32[]{:S(2)}) copy-start(f32[512]{0:T(512)} %param.23) | copy-start | bytes 6148
  21.3 12.8 %copy-start.5 = (f32[512]{0:T(512)S(1)}, f32[512]{0:T(512)}, u32[]{:S(2)}) copy-start(f32[512]{0:T(512)} %param.24) | copy-start | bytes 6148
  27.6 27.2 %copy-start.2 = (bf16[4,128,512]{2,1,0:T(8,128)(2,1)}, bf16[4,128,512]{2,1,0:T(8,128)(2,1)S(1)}, u32[]{:S(2)}) copy-start(bf16[4,128,512]{2,1,0:T(8,128)(2,1)S(1)} %all-to-all-done.1.res_ref) | copy-start | bytes 1572868
  27.6 20.3 %all-to-all-start = ((f32[4,136,256]{2,1,0:T(8,128)}), f32[4,136,256]{2,1,0:T(8,128)S(1)}, u32[]{:S(2)}, u32[]{:S(2)}) async-start(f32[4,136,256]{2,1,0:T(8,128)} %pad_maximum_fusion), calls=%async_computation | async-start | bytes 1114112 | tf_op jit(solution)/shard_map/all_to_all | solution.py:347
  33.4 27.1 %copy-start.3 = (s32[128,2]{1,0:T(8,128)}, s32[128,2]{1,0:T(8,128)S(1)}, u32[]{:S(2)}) copy-start(s32[128,2]{1,0:T(8,128)S(1)} %multiply_add_fusion.slots_ref) | copy-start | bytes 3076
  47.9 7.0 %copy-start.1 = (f32[4,136,256]{2,1,0:T(8,128)}, f32[4,136,256]{2,1,0:T(8,128)S(1)}, u32[]{:S(2)}) copy-start(f32[4,136,256]{2,1,0:T(8,128)S(1)} %all-to-all-done.conv_ref) | copy-start | bytes 1671172
Sparse Core Ops, SparseCore 0:
  8.9 45.9 all-gather.2

commit v3 on v2

--- a/solution.py
+++ b/solution.py
@@ -7,12 +7,6 @@
 from jax.sharding import PartitionSpec as P
 
 eps = 1e-06
-
-
-def passed_along(value, axis, steps):
-    count = lax.axis_size(axis)
-    leading, last = (max(0, -steps), min(count, count - steps))
-    return lax.ppermute(value, axis, [(source, source + steps) for source in range(leading, last)])
 
 
 def sigmoid(v):
@@ -63,22 +57,156 @@
             ).astype(jnp.bfloat16)
 
 
-def mix(conv, residual, weight, slots, slot_num):
+def front_kernel(
+    reach,
+    value_ref,
+    gate_ref,
+    tap_ref,
+    extra_ref,
+    res_ref,
+    weight_ref,
+    slots_ref,
+    middle_ref,
+    out_ref,
+    tail_value,
+    tail_gate,
+    gated,
+    message,
+    conv_rows,
+    res_rows,
+    weight_all,
+    h_send,
+    h_recv,
+    w_send,
+    w_recv,
+    r_send,
+    r_recv,
+    c_send,
+    c_recv,
+    own_sem,
+):
+    blocks, rows, columns = res_ref.shape
+    row_count = value_ref.shape[0]
+    pad = tail_value.shape[0]
+    me, mine = lax.axis_index("sp"), lax.axis_index("tp")
+    seq_num = lax.axis_size("sp")
+    partner = mine + 1 - 2 * lax.rem(mine, 2)
+    counter = lax.rem(mine + blocks // 2, blocks)
+    diagonal = lax.rem(partner + blocks // 2, blocks)
+    after = {"sp": lax.rem(me + 1, seq_num)}
+    before = {"sp": lax.rem(me + seq_num - 1, seq_num)}
+    mates = ((1, counter), (2, diagonal), (0, partner))
+
+    barrier = pltpu.get_barrier_semaphore()
+    for device in [{"tp": mate} for _, mate in mates] + [before, after]:
+        pl.semaphore_signal(barrier, inc=1, device_id=device, device_id_type=pl.DeviceIdType.MESH)
+    pl.semaphore_wait(barrier, len(mates) + 2)
+
+    def remote(src, dst, send, recv, device):
+        copy = pltpu.make_async_remote_copy(
+            src_ref=src,
+            dst_ref=dst,
+            send_sem=send,
+            recv_sem=recv,
+            device_id=device,
+            device_id_type=pl.DeviceIdType.MESH,
+        )
+        copy.start()
+        return copy
+
+    last = pl.ds(row_count - pad, pad)
+    halo = [
+        remote(value_ref.at[last], tail_value, h_send.at[0], h_recv.at[0], after),
+        remote(gate_ref.at[last], tail_gate, h_send.at[1], h_recv.at[1], after),
+    ]
+    res_copies = [
+        remote(res_ref.at[mate], res_rows.at[mine], r_send.at[j], r_recv.at[j], {"tp": mate})
+        for j, mate in mates
+    ]
+    across = remote(weight_ref, weight_all.at[mine], w_send.at[0], w_recv.at[0], {"tp": counter})
+    beside = remote(weight_ref, weight_all.at[mine], w_send.at[1], w_recv.at[1], {"tp": partner})
+    own = [
+        pltpu.make_async_copy(weight_ref, weight_all.at[mine], own_sem.at[0]),
+        pltpu.make_async_copy(res_ref.at[mine], res_rows.at[mine], own_sem.at[1]),
+    ]
+    for copy in own:
+        copy.start()
+
+    def gate_of(value, gate):
+        return value.astype(jnp.float32) * sigmoid(gate.astype(jnp.float32))
+
+    gated[pad:, :] = gate_of(value_ref[...], gate_ref[...])
+    for copy in halo:
+        copy.wait()
+    first = gate_of(tail_value[...], tail_gate[...])
+    gated[:pad, :] = jnp.where(me > 0, first, jnp.zeros_like(first))
+    for b in range(blocks):
+        for low in range(b * rows, (b + 1) * rows, rows // 2):
+            part = jnp.zeros((rows // 2, value_ref.shape[1]), jnp.float32)
+            for tap in range(reach + 1):
+                begin = low + pad - reach + tap
+                part = part + tap_ref[tap : tap + 1, :] * gated[begin : begin + rows // 2, :]
+            message[b, low - b * rows : low - b * rows + rows // 2, :] = part
+        message[b, rows:, :] = extra_ref[...]
+    conv_copies = [
+        remote(message.at[mate], conv_rows.at[mine], c_send.at[j], c_recv.at[j], {"tp": mate})
+        for j, mate in mates
+    ]
+    own_conv = pltpu.make_async_copy(message.at[mine], conv_rows.at[mine], own_sem.at[2])
+    own_conv.start()
+    across.wait_recv()
+    passed = remote(
+        weight_all.at[counter], weight_all.at[counter], w_send.at[2], w_recv.at[2], {"tp": partner}
+    )
+    for copy in own + [own_conv]:
+        copy.wait()
+    for copy in res_copies + conv_copies + [beside, passed]:
+        copy.wait()
+    across.wait_send()
+    mix_kernel(rows, conv_rows, res_rows, weight_all, slots_ref, middle_ref, out_ref)
+
+
+def front(value, gate, taps, extras, residual, weight, slots, slot_num):
     blocks, rows, columns = residual.shape
+    row_count, width = value.shape
+    reach = taps.shape[0] - 1
+    pad = reach + -reach % 16
+    vmem, anywhere = pl.BlockSpec(memory_space=pltpu.VMEM), pl.BlockSpec(memory_space=pl.ANY)
+    dma = pltpu.SemaphoreType.DMA
+    sent = (blocks, rows + extras.shape[0], width)
     return pl.pallas_call(
-        functools.partial(mix_kernel, rows),
+        functools.partial(front_kernel, reach),
         out_shape=(
             jax.ShapeDtypeStruct(residual.shape, jnp.bfloat16),
             jax.ShapeDtypeStruct((slot_num, blocks * columns), jnp.bfloat16),
         ),
-        in_specs=[pl.BlockSpec(memory_space=pltpu.VMEM)] * 4,
-        out_specs=[pl.BlockSpec(memory_space=pltpu.VMEM)] * 2,
+        in_specs=[vmem, vmem, vmem, vmem, vmem, anywhere, vmem],
+        out_specs=[vmem, vmem],
+        scratch_shapes=[
+            pltpu.VMEM((pad, width), jnp.bfloat16),
+            pltpu.VMEM((pad, width), jnp.bfloat16),
+            pltpu.VMEM((pad + row_count, width), jnp.float32),
+            pltpu.VMEM(sent, jnp.float32),
+            pltpu.VMEM(sent, jnp.float32),
+            pltpu.VMEM(residual.shape, jnp.bfloat16),
+            pltpu.VMEM((blocks,) + weight.shape, jnp.bfloat16),
+            dma((2,)),
+            dma((2,)),
+            dma((3,)),
+            dma((3,)),
+            dma((3,)),
+            dma((3,)),
+            dma((3,)),
+            dma((3,)),
+            dma((3,)),
+        ],
+        compiler_params=pltpu.CompilerParams(collective_id=1, has_side_effects=True),
         cost_estimate=pl.CostEstimate(
-            flops=2 * rows * weight.size + 2 * slot_num * rows * blocks * columns,
-            bytes_accessed=2 * weight.size + 4 * conv.size,
+            flops=2 * rows * weight.size * blocks,
+            bytes_accessed=8 * weight.size,
             transcendentals=0,
         ),
-    )(conv, residual, weight, slots)
+    )(value, gate, taps, extras, residual, weight, slots)
 
 
 def expert_kernel(
@@ -318,33 +446,10 @@
     slot_num = seq_devices * capacity
     my_index = lax.axis_index("tp")
 
-    out_all = lax.all_gather(out_weight, "tp", axis=0, tiled=False)
-
-    tails = jnp.concatenate(
-        [conv_value[row_count - reach_rows :], conv_gate[row_count - reach_rows :]], axis=1
-    )
-    previous = passed_along(tails, "sp", 1)
-    res_rows = lax.all_to_all(
-        residual.reshape(tp_devices, quarter, columns), "tp", split_axis=0, concat_axis=0, tiled=True
-    )
-    values = jnp.concatenate([previous[:, :width], conv_value], axis=0).astype(jnp.float32)
-    gate_pre = jnp.concatenate([previous[:, width:], conv_gate], axis=0).astype(jnp.float32)
-    gated = values * jax.nn.sigmoid(gate_pre)
-    convolved = jnp.zeros((row_count, width), jnp.float32)
-    for tap_index in range(reach_rows + 1):
-        convolved = convolved + conv_weight[tap_index] * gated[tap_index : tap_index + row_count]
     extras = jnp.concatenate(
         [conv_gain[None], conv_shift[None], mix_gain.reshape(-1, width)], axis=0
     )
     extras = jnp.pad(extras, ((0, -extras.shape[0] % 8), (0, 0)))
-    message = jnp.concatenate(
-        [
-            convolved.reshape(tp_devices, quarter, width),
-            jnp.broadcast_to(extras[None], (tp_devices,) + extras.shape),
-        ],
-        axis=1,
-    )
-    conv_rows = lax.all_to_all(message, "tp", split_axis=0, concat_axis=0, tiled=True)
 
     own = lax.dynamic_slice_in_dim(expert_ids, my_index * quarter, quarter, 0)
     flat = own.reshape(-1)
@@ -355,7 +460,16 @@
     rank = jnp.sum(before * onehot.astype(jnp.float32), axis=-1).astype(jnp.int32)
     slots = (flat * capacity + rank).reshape(quarter, 2)
 
-    middle, outgoing = mix(conv_rows, res_rows, out_all, slots.T, slot_num)
+    middle, outgoing = front(
+        conv_value,
+        conv_gate,
+        conv_weight,
+        extras,
+        residual.reshape(tp_devices, quarter, columns),
+        out_weight,
+        slots.T,
+        slot_num,
+    )
     gates = jnp.stack([group_weight, score_gap], axis=1)
     own_gates = lax.dynamic_slice_in_dim(gates, my_index * quarter, quarter, 0)
     return expert(

time: 205 us -> 186 us (0.907)
  Pallas kernels: 140 us -> 178 us
  waiting for transfers between devices: 24 us -> 0 us
  between operations: 13.5 us -> 0.07 us
  starting transfers between devices: 13 us -> 0 us
  other arithmetic: 5.04 us -> 2.06 us
  local copies, waits for them, and re-layouts: 7.83 us -> 5.04 us
    pallas_call x1, Pallas kernels: 5.63 us -> 42 us  [front(): pl.pallas_call(functools.partial(front_kernel, reach), out_shape=(jax.Sha...]
    all_to_all x2 -> x0, waiting for transfers between devices: 16.3 us -> none  [the longest x1 13 us: shards(): lax.all_to_all(message, 'tp', split_axis=0, concat_axis=0, tiled=True)]
    all_to_all x2 -> x0, starting transfers between devices: 9.86 us -> none  [the longest x1 5.45 us: shards(): lax.all_to_all(message, 'tp', split_axis=0, concat_axis=0, tiled=True)]
    all_gather x1 -> x0, waiting for transfers between devices: 6.96 us -> none  [shards(): out_all = lax.all_gather(out_weight, 'tp', axis=0, tiled=False)]
    slice x5 -> x0, local copies, waits for them, and re-layouts: 3.45 us -> none  [the longest x2 1.99 us: shards(): conv_weight[tap_index] * gated[tap_index:tap_index + row_count]]
    ppermute x1 -> x0, starting transfers between devices: 3.12 us -> none  [passed_along(): lax.ppermute(value, axis, [(source, source + steps) for source in range(l...]
    add x1 -> x0, other arithmetic: 2.09 us -> none  [shards(): convolved + conv_weight[tap_index] * gated[tap_index:tap_index + row_count]]
  transfers between devices with their start and end apart: 4 -> 0, of which waited for: 3 -> 0; matrix products, arithmetic and copies ran while one was open for 5% -> 0% of each run, Pallas kernels for 0% -> 0%
where the time goes in v3:
time: 186 us; the launch traced here: 185 us
  Pallas kernels  178 us (96%)
  local copies, waits for them, and re-layouts  5.04 us (3%)
  other arithmetic  2.06 us (1%)
    pallas_call x1, Pallas kernels, expert(): pl.pallas_call(functools.partial(expert_kernel, seq_num), out_shape=jax.S...  136 us
    pallas_call x1, Pallas kernels, front(): pl.pallas_call(functools.partial(front_kernel, reach), out_shape=(jax.Sha...  42 us

profile of v3, /device:TPU:17, one launch (start us, length us, event | category | flops | bytes accessed | tf_op | source)
XLA Modules:
  0.0 185.3 jit_solution(5724287379856814152)
XLA Ops:
  0.0 0.0 copy-start
  0.0 0.7 copy-done
  0.7 0.7 fusion.3
  1.4 0.7 reshape.11
  2.1 1.3 select_maximum_fusion.extra_ref
  3.4 0.1 copy.24
  3.5 0.1 eq.15
  3.7 0.2 fusion
  3.9 0.1 convert_element_type.19
  4.1 0.0 copy-start.1
  4.1 0.7 copy.22.slots_ref
  4.7 0.7 copy.25.gates_ref
  5.5 42.0 %shard_map.136 = (bf16[4,128,512]{2,1,0:T(8,128)(2,1)}, bf16[512,2048]{1,0:T(8,128)(2,1)}) custom-call(bf16[512,256]{1,0:T(8,128)(2,1)} %value_ref.1, bf16[512,256]{1,0:T(8,128)(2,1)} %gate_ref.1, f32[31,256]{1,0:T(8,128)} %tap_ref.1, f32[8,256]{1,0:T(8,128)} %select_maximum_fusion.extra_ref, bf16[4,128,512]{2,1,0:T(8,128)(2,1)} %bitcast.9, ...), custom_call_target="tpu_custom_call" | custom-call | flops 536870912 | bytes 4194304 | tf_op jit(solution)/shard_map/pallas_call | solution.py:177
  47.5 0.0 copy-done.1
  47.5 135.9 %shard_map.137 = bf16[512,512]{1,0:T(8,128)(2,1)} custom-call(bf16[512,2048]{1,0:T(8,128)(2,1)} %get-tuple-element.7.x_ref, bf16[2048,256]{1,0:T(8,128)(2,1)} %bitcast.15, bf16[2048,256]{1,0:T(8,128)(2,1)} %bitcast.16, bf16[256,2048]{1,0:T(8,128)(2,1)} %bitcast.17, bf16[4,128,512]{2,1,0:T(8,128)(2,1)} %get-tuple-element.8.middle_ref, s32[128,2]{1,0:T(8,128)} %copy-done.1, ...), custom_call_target="tpu_custom_call" | custom-call | flops 6442450944 | bytes 12582912 | tf_op jit(solution)/shard_map/pallas_call | solution.py:389
  183.4 1.9 %copy.27 = bf16[512,512]{1,0:T(8,128)(2,1)} copy(bf16[512,512]{1,0:T(8,128)(2,1)} %shard_map.137) | data formatting | bytes 1048576
  (3 shorter events, 0.0 us)
Async XLA Ops:
  0.0 0.7 copy-start
  4.1 43.4 %copy-start.1 = (s32[128,2]{1,0:T(8,128)}, s32[128,2]{1,0:T(8,128)S(1)}, u32[]{:S(2)}) copy-start(s32[128,2]{1,0:T(8,128)S(1)} %multiply_add_fusion.slots_ref) | copy-start | bytes 3076
